TPU v7x, 32 devices: a whole 2x2x4 slice. The times are simulated.
32 devices in a mesh: sp: 4 (over y, x), tp: 8 (over z, core).
Axes of the slice: x: 2, y: 2, z: 4, core: 2. Of those that a mesh axis runs over, the one named last changes fastest.
Arguments:
- tokens: bfloat16 [512, 1024], P('sp', 'tp'), may hold values from -6 to 6
- segment_ids: int32 [512], P('sp'), may hold values from 0 to 7, never falling along the last dimension, each value on 1 to 128 neighbouring positions
- gains: float32 [2, 1024], replicated, may hold values from 0.1 to 1.9
- w_query: bfloat16 [2, 1024, 1024], P(None, 'sp', 'tp'), may hold values from -0.1875 to 0.1875
- w_key: bfloat16 [2, 1024, 1024], P(None, 'sp', 'tp'), may hold values from -0.1875 to 0.1875
- w_value: bfloat16 [2, 1024, 1024], P(None, 'sp', 'tp'), may hold values from -0.1875 to 0.1875
- w_out: bfloat16 [2, 1024, 1024], P(None, 'tp', 'sp'), may hold values from -0.1875 to 0.1875
- rel_bias: float32 [2, 16, 5, 9], P(None, 'tp'), may hold values from -4 to 4
Outputs:
- mixed_out: bfloat16 [512, 1024], P('sp', 'tp')
Inputs may be any that keep to these rules, and one draw needn't show every extreme that they name: `segment_ids`: segment numbers never fall along the token order; each document has 1 to 128 positions.
All inputs are finite; a program needn't handle non-finite values.
Results may differ from a plain program's by a relative error of at most 0.03.
Values may be sent and summed in bfloat16 or wider, within the bound.
A program may use at most 64 MiB of HBM per device.

v0:
```python
import functools

import jax
import jax.numpy as jnp
from jax import lax
from jax.experimental import pallas as pl
from jax.experimental.pallas import tpu as pltpu
from jax.sharding import PartitionSpec as P

MESH = pl.DeviceIdType.MESH

HEAD_DIM = 64
GRID_W = 32
REACH_R = 2
REACH_C = 4

norm_eps = 1e-06
masked_score = -1e30
F32 = jnp.float32
BF16 = jnp.bfloat16


def remote(src, dst, send_sem, recv_sem, where):
    return pltpu.make_async_remote_copy(
        src_ref=src, dst_ref=dst, send_sem=send_sem, recv_sem=recv_sem, device_id=where, device_id_type=MESH
    )


def kernel(
    n_sp, n_tp, tok, seg, gains, wq, wk, wv, wo, rel, out,
    xbuf, wbuf, wobuf, kvbuf, part, rsbuf, cur, docbuf, gbuf, relbuf, biasbuf,
    local_sem, x_send, x_recv, w_send, w_recv, o_send, o_recv, h_send, h_recv, r_send, r_recv, d_send, d_recv,
):
    s, t = lax.axis_index("sp"), lax.axis_index("tp")
    layers = wbuf.shape[0]
    rows, feat = tok.shape
    heads = feat // HEAD_DIM
    halo = REACH_R * GRID_W
    keys = rows + 2 * halo
    grid_rows = rows // GRID_W
    prev, following = lax.rem(s + n_sp - 1, n_sp), lax.rem(s + 1, n_sp)
    tp_peers = [lax.rem(t + k, n_tp) for k in range(1, n_tp)]
    sp_peers = [lax.rem(s + k, n_sp) for k in range(1, n_sp)]

    local = [
        pltpu.make_async_copy(seg, docbuf.at[1], local_sem.at[0]),
        pltpu.make_async_copy(gains, gbuf, local_sem.at[1]),
        pltpu.make_async_copy(rel, relbuf, local_sem.at[2]),
        pltpu.make_async_copy(tok, xbuf.at[0, t], local_sem.at[3]),
    ]
    weights = (wq, wk, wv)
    for l in range(layers):
        for j in range(3):
            local.append(pltpu.make_async_copy(weights[j].at[l], wbuf.at[l, j, s], local_sem.at[4 + 4 * l + j]))
        local.append(pltpu.make_async_copy(wo.at[l], wobuf.at[l, s], local_sem.at[7 + 4 * l]))
    for copy in local:
        copy.start()

    barrier = pltpu.get_barrier_semaphore()
    for peer in tp_peers:
        pl.semaphore_signal(barrier, inc=1, device_id=(s, peer), device_id_type=MESH)
    for peer in sp_peers:
        pl.semaphore_signal(barrier, inc=1, device_id=(peer, t), device_id_type=MESH)
    pl.semaphore_wait(barrier, n_tp + n_sp - 2)

    def x_copy(l, slot, peer):
        return remote(tok if l == 0 else cur, xbuf.at[l, slot], x_send.at[l, peer], x_recv.at[l, slot], (s, peer))

    def w_copy(l, j, slot, peer):
        return remote(weights[j].at[l], wbuf.at[l, j, slot], w_send.at[l, j, peer], w_recv.at[l, j, slot], (peer, t))

    def o_copy(l, slot, peer):
        return remote(wo.at[l], wobuf.at[l, slot], o_send.at[l, peer], o_recv.at[l, slot], (peer, t))

    def halo_copies(l):
        up = remote(
            kvbuf.at[l, :, pl.ds(rows, halo)], kvbuf.at[l, :, pl.ds(0, halo)],
            h_send.at[l, 0], h_recv.at[l, 0], (following, t),
        )
        down = remote(
            kvbuf.at[l, :, pl.ds(halo, halo)], kvbuf.at[l, :, pl.ds(rows + halo, halo)],
            h_send.at[l, 1], h_recv.at[l, 1], (prev, t),
        )
        return up, down

    def r_copy(l, peer, slot):
        return remote(part.at[l, peer], rsbuf.at[l, slot], r_send.at[l, peer], r_recv.at[l, slot], (s, peer))

    docs = (
        remote(seg, docbuf.at[0], d_send.at[0], d_recv.at[0], (following, t)),
        remote(seg, docbuf.at[2], d_send.at[1], d_recv.at[1], (prev, t)),
    )
    for peer in tp_peers:
        x_copy(0, t, peer).start()
    for j in (1, 2, 0):
        for peer in sp_peers:
            w_copy(0, j, s, peer).start()
    for copy in docs:
        copy.start()

    local[0].wait()
    local[1].wait()
    local[2].wait()
    for copy in docs:
        copy.wait_recv()

    doc_before = jnp.where(s == 0, -1, docbuf[0])
    doc_after = jnp.where(s == n_sp - 1, -1, docbuf[2])
    doc_own = docbuf[1]
    doc_keys = jnp.concatenate([doc_before[:, rows - halo :], doc_own, doc_after[:, :halo]], axis=1).astype(F32)
    doc_query = jnp.transpose(jnp.broadcast_to(doc_own.astype(F32), (rows, rows)))[:, :1]
    lane = lax.broadcasted_iota(jnp.int32, (1, keys), 1)
    key_row = lane // GRID_W
    key_col = lax.rem(lax.broadcasted_iota(jnp.int32, (GRID_W, keys), 1), GRID_W)
    col_off = key_col - lax.broadcasted_iota(jnp.int32, (GRID_W, keys), 0)
    for l in range(layers):
        for h in range(heads):
            table = relbuf[l, h]
            cells = [
                [jnp.broadcast_to(table[a : a + 1, b : b + 1], (1, keys)) for b in range(2 * REACH_C + 1)]
                for a in range(2 * REACH_R + 1)
            ]
            for r in range(grid_rows):
                block = jnp.full((GRID_W, keys), masked_score, F32)
                for b in range(2 * REACH_C + 1):
                    line = jnp.full((1, keys), masked_score, F32)
                    for a in range(2 * REACH_R + 1):
                        line = jnp.where(key_row == r + a, cells[a][b], line)
                    block = jnp.where(col_off == b - REACH_C, line, block)
                same = doc_query[r * GRID_W : (r + 1) * GRID_W] == doc_keys
                biasbuf[l, pl.ds(h * rows + r * GRID_W, GRID_W)] = jnp.where(same, block, masked_score)

    local[3].wait()
    for copy in local[4:]:
        copy.wait()

    for l in range(layers):
        for peer in tp_peers:
            x_copy(l, peer, peer).wait_recv()
        pieces = [xbuf[l, i].astype(F32) for i in range(n_tp)]
        square = sum(piece * piece for piece in pieces)
        mean_sq = jnp.sum(square, axis=-1, keepdims=True) / (n_tp * feat)
        inv = lax.rsqrt(mean_sq + norm_eps)
        gain = gbuf[l : l + 1]
        normed = jnp.concatenate(
            [(piece * inv * gain[:, i * feat : (i + 1) * feat]).astype(BF16) for i, piece in enumerate(pieces)],
            axis=1,
        )

        def project(j):
            for peer in sp_peers:
                w_copy(l, j, peer, peer).wait_recv()
            weight = wbuf[l, j].reshape(n_tp * feat, feat)
            return jnp.dot(normed, weight, preferred_element_type=F32).astype(BF16)

        kvbuf[l, 0, pl.ds(halo, rows)] = project(1)
        kvbuf[l, 1, pl.ds(halo, rows)] = project(2)
        halos = halo_copies(l)
        for copy in halos:
            copy.start()
        if l == 0:
            for peer in sp_peers:
                o_copy(0, s, peer).start()
        query = project(0) * jnp.asarray(HEAD_DIM**-0.5, BF16)
        head_of = lax.broadcasted_iota(jnp.int32, (rows, feat), 1) // HEAD_DIM
        query = jnp.concatenate([jnp.where(head_of == h, query, jnp.zeros_like(query)) for h in range(heads)], axis=0)
        for copy in halos:
            copy.wait_recv()
        if l + 1 < layers:
            for j in (1, 2, 0):
                for peer in sp_peers:
                    w_copy(l + 1, j, s, peer).start()
        scores = lax.dot_general(query, kvbuf[l, 0], (((1,), (1,)), ((), ())), preferred_element_type=F32)
        scores = scores + biasbuf[l]
        weight = jnp.exp(scores - jnp.max(scores, axis=-1, keepdims=True))
        total = jnp.sum(weight, axis=-1, keepdims=True)
        blended = jnp.dot(weight.astype(BF16), kvbuf[l, 1], preferred_element_type=F32) / total
        attended = blended[:rows]
        for h in range(1, heads):
            attended = jnp.where(head_of == h, blended[h * rows : (h + 1) * rows], attended)
        attended = attended.astype(BF16)

        for peer in sp_peers:
            o_copy(l, peer, peer).wait_recv()
        if l + 1 < layers:
            for peer in sp_peers:
                o_copy(l + 1, s, peer).start()
        width = wobuf.shape[3]
        for i in range(n_sp):
            piece = jnp.dot(attended, wobuf[l, i], preferred_element_type=F32).astype(BF16)
            for j in range(width // feat):
                part[l, i * (width // feat) + j] = piece[:, j * feat : (j + 1) * feat]
        for peer in tp_peers:
            r_copy(l, peer, t).start()
        summed = part[l, t].astype(F32)
        for peer in tp_peers:
            r_copy(l, peer, peer).wait_recv()
            summed = summed + rsbuf[l, peer].astype(F32)
        if l + 1 < layers:
            cur[...] = summed.astype(BF16)
            for peer in tp_peers:
                x_copy(l + 1, t, peer).start()
            xbuf[l + 1, t] = summed.astype(BF16)
        else:
            out[...] = summed.astype(BF16)

    for copy in docs:
        copy.wait_send()
    for l in range(layers):
        for peer in tp_peers:
            x_copy(l, t, peer).wait_send()
            r_copy(l, peer, t).wait_send()
        for peer in sp_peers:
            for j in range(3):
                w_copy(l, j, s, peer).wait_send()
            o_copy(l, s, peer).wait_send()
        for copy in halo_copies(l):
            copy.wait_send()


def on_device(n_sp, n_tp, tokens, segment_ids, gains, w_query, w_key, w_value, w_out, rel_bias):
    rows, feat = tokens.shape
    layers, depth, _ = w_query.shape
    width = w_out.shape[2]
    halo = REACH_R * GRID_W
    keys = rows + 2 * halo
    heads = feat // HEAD_DIM
    dma = pltpu.SemaphoreType.DMA
    anywhere = pl.BlockSpec(memory_space=pl.ANY)
    return pl.pallas_call(
        functools.partial(kernel, n_sp, n_tp),
        out_shape=jax.ShapeDtypeStruct((rows, feat), BF16),
        in_specs=[anywhere] * 8,
        out_specs=pl.BlockSpec(memory_space=pltpu.VMEM),
        scratch_shapes=[
            pltpu.VMEM((layers, n_tp, rows, feat), BF16),
            pltpu.VMEM((layers, 3, n_sp, depth, feat), BF16),
            pltpu.VMEM((layers, n_sp, feat, width), BF16),
            pltpu.VMEM((layers, 2, keys, feat), BF16),
            pltpu.VMEM((layers, n_tp, rows, feat), BF16),
            pltpu.VMEM((layers, n_tp, rows, feat), BF16),
            pltpu.VMEM((rows, feat), BF16),
            pltpu.VMEM((3, 1, rows), jnp.int32),
            pltpu.VMEM(gains.shape, F32),
            pltpu.VMEM(rel_bias.shape, F32),
            pltpu.VMEM((layers, heads * rows, keys), F32),
            dma((4 + 4 * layers,)),
            dma((layers, n_tp)),
            dma((layers, n_tp)),
            dma((layers, 3, n_sp)),
            dma((layers, 3, n_sp)),
            dma((layers, n_sp)),
            dma((layers, n_sp)),
            dma((layers, 2)),
            dma((layers, 2)),
            dma((layers, n_tp)),
            dma((layers, n_tp)),
            dma((2,)),
            dma((2,)),
        ],
        compiler_params=pltpu.CompilerParams(
            collective_id=0, has_side_effects=True, vmem_limit_bytes=48 * 1024 * 1024
        ),
    )(tokens, segment_ids.reshape(1, rows), gains, w_query, w_key, w_value, w_out, rel_bias)


def solution(mesh):
    return jax.shard_map(
        functools.partial(on_device, mesh.shape["sp"], mesh.shape["tp"]),
        mesh=mesh,
        in_specs=(
            P("sp", "tp"),
            P("sp"),
            P(),
            P(None, "sp", "tp"),
            P(None, "sp", "tp"),
            P(None, "sp", "tp"),
            P(None, "tp", "sp"),
            P(None, "tp", None, None),
        ),
        out_specs=P("sp", "tp"),
        check_vma=False,
    )
```

profile of v0, /device:TPU:1, one launch (start us, length us, event | category | flops | bytes accessed | tf_op | source)
XLA Modules:
  0.0 55.3 jit_solution(2585999808389206716)
XLA Ops:
  0.0 0.0 copy-start.5
  0.0 0.0 copy-start.6
  0.0 0.7 %copy.9.rel = f32[2,2,5,9]{3,2,1,0:T(8,128)S(1)} copy(f32[2,2,5,9]{3,1,2,0:T(2,128)} %param.15) | data formatting | bytes 1440 | tf_op args[7]
  0.7 0.0 copy-done.5
  0.7 0.0 copy-done.6
  0.7 0.0 copy-start
  0.7 0.9 %copy-done = bf16[2,256,128]{2,1,0:T(8,128)(2,1)S(1)} copy-done((bf16[2,256,128]{2,1,0:T(8,128)(2,1)S(1)}, bf16[2,256,128]{2,1,0:T(8,128)(2,1)}, u32[]{:S(2)}) %copy-start) | copy-done | bytes 131096
  1.6 0.0 copy-start.1
  1.6 0.9 %copy-done.1 = bf16[2,256,128]{2,1,0:T(8,128)(2,1)S(1)} copy-done((bf16[2,256,128]{2,1,0:T(8,128)(2,1)S(1)}, bf16[2,256,128]{2,1,0:T(8,128)(2,1)}, u32[]{:S(2)}) %copy-start.1) | copy-done | bytes 131096
  2.6 0.0 copy-start.2
  2.6 0.9 %copy-done.2 = bf16[2,256,128]{2,1,0:T(8,128)(2,1)S(1)} copy-done((bf16[2,256,128]{2,1,0:T(8,128)(2,1)S(1)}, bf16[2,256,128]{2,1,0:T(8,128)(2,1)}, u32[]{:S(2)}) %copy-start.2) | copy-done | bytes 131096
  3.5 0.0 copy-start.3
  3.5 0.9 %copy-done.3 = bf16[2,128,256]{2,1,0:T(8,128)(2,1)S(1)} copy-done((bf16[2,128,256]{2,1,0:T(8,128)(2,1)S(1)}, bf16[2,128,256]{2,1,0:T(8,128)(2,1)}, u32[]{:S(2)}) %copy-start.3) | copy-done | bytes 131096
  4.4 0.0 copy-start.4
  4.4 0.8 %copy-done.4 = bf16[128,128]{1,0:T(8,128)(2,1)S(1)} copy-done((bf16[128,128]{1,0:T(8,128)(2,1)S(1)}, bf16[128,128]{1,0:T(8,128)(2,1)}, u32[]{:S(2)}) %copy-start.4) | copy-done | bytes 32792
  5.1 49.5 %shard_map.82 = bf16[128,128]{1,0:T(8,128)(2,1)S(1)} custom-call(bf16[128,128]{1,0:T(8,128)(2,1)S(1)} %copy-done.4, s32[1,128]{1,0:T(1,128)S(1)} %bitcast.1, f32[2,1024]{1,0:T(2,128)S(1)} %copy-done.5, bf16[2,256,128]{2,1,0:T(8,128)(2,1)S(1)} %copy-done, bf16[2,256,128]{2,1,0:T(8,128)(2,1)S(1)} %copy-done.1, bf16[2,256,128]{2,1,0:T(8,128)(2,1)S(1)} %copy-done.2, ...), custom_call_target="tpu_custom_call" | custom-call | tf_op jit(solution)/shard_map/pallas_call | solution.py:230
  54.6 0.6 %copy.11 = bf16[128,128]{1,0:T(8,128)(2,1)} copy(bf16[128,128]{1,0:T(8,128)(2,1)S(1)} %shard_map.82) | data formatting | bytes 65536
Async XLA Ops:
  0.0 0.7 %copy-start.5 = (f32[2,1024]{1,0:T(2,128)S(1)}, f32[2,1024]{1,0:T(2,128)}, u32[]{:S(2)}) copy-start(f32[2,1024]{1,0:T(2,128)} %gains.1) | copy-start | bytes 24580
  0.0 0.7 %copy-start.6 = (s32[128]{0:T(128)S(1)}, s32[128]{0:T(128)}, u32[]{:S(2)}) copy-start(s32[128]{0:T(128)} %param.9) | copy-start | bytes 1540
  0.7 0.9 %copy-start = (bf16[2,256,128]{2,1,0:T(8,128)(2,1)S(1)}, bf16[2,256,128]{2,1,0:T(8,128)(2,1)}, u32[]{:S(2)}) copy-start(bf16[2,256,128]{2,1,0:T(8,128)(2,1)} %wq.1) | copy-start | bytes 393220
  1.6 0.9 %copy-start.1 = (bf16[2,256,128]{2,1,0:T(8,128)(2,1)S(1)}, bf16[2,256,128]{2,1,0:T(8,128)(2,1)}, u32[]{:S(2)}) copy-start(bf16[2,256,128]{2,1,0:T(8,128)(2,1)} %wk.1) | copy-start | bytes 393220
  2.6 0.9 %copy-start.2 = (bf16[2,256,128]{2,1,0:T(8,128)(2,1)S(1)}, bf16[2,256,128]{2,1,0:T(8,128)(2,1)}, u32[]{:S(2)}) copy-start(bf16[2,256,128]{2,1,0:T(8,128)(2,1)} %wv.1) | copy-start | bytes 393220
  3.5 0.9 %copy-start.3 = (bf16[2,128,256]{2,1,0:T(8,128)(2,1)S(1)}, bf16[2,128,256]{2,1,0:T(8,128)(2,1)}, u32[]{:S(2)}) copy-start(bf16[2,128,256]{2,1,0:T(8,128)(2,1)} %wo.1) | copy-start | bytes 393220
  4.4 0.8 %copy-start.4 = (bf16[128,128]{1,0:T(8,128)(2,1)S(1)}, bf16[128,128]{1,0:T(8,128)(2,1)}, u32[]{:S(2)}) copy-start(bf16[128,128]{1,0:T(8,128)(2,1)} %tok.1) | copy-start | bytes 98308
where the time goes:
time: 55.5 us; the launch traced here: 55.3 us
  Pallas kernels  49.5 us (89%)
  local copies, waits for them, and re-layouts  5.73 us (10%)
    pallas_call x1, Pallas kernels, on_device(): pl.pallas_call(functools.partial(kernel, n_sp, n_tp), out_shape=jax.Shape...  49.5 us
    unnamed x16, local copies, waits for them, and re-layouts  5.73 us

commit v1 on v0

--- a/solution.py
+++ b/solution.py
@@ -115,9 +115,8 @@
     col_off = key_col - lax.broadcasted_iota(jnp.int32, (GRID_W, keys), 0)
     for l in range(layers):
         for h in range(heads):
-            table = relbuf[l, h]
             cells = [
-                [jnp.broadcast_to(table[a : a + 1, b : b + 1], (1, keys)) for b in range(2 * REACH_C + 1)]
+                [jnp.broadcast_to(relbuf[l, a, h : h + 1, b : b + 1], (1, keys)) for b in range(2 * REACH_C + 1)]
                 for a in range(2 * REACH_R + 1)
             ]
             for r in range(grid_rows):
@@ -225,8 +224,9 @@
     halo = REACH_R * GRID_W
     keys = rows + 2 * halo
     heads = feat // HEAD_DIM
+    rel_by_row = jnp.transpose(rel_bias, (0, 2, 1, 3))
     dma = pltpu.SemaphoreType.DMA
-    anywhere = pl.BlockSpec(memory_space=pl.ANY)
+    anywhere = pl.BlockSpec(memory_space=pltpu.HBM)
     return pl.pallas_call(
         functools.partial(kernel, n_sp, n_tp),
         out_shape=jax.ShapeDtypeStruct((rows, feat), BF16),
@@ -242,7 +242,7 @@
             pltpu.VMEM((rows, feat), BF16),
             pltpu.VMEM((3, 1, rows), jnp.int32),
             pltpu.VMEM(gains.shape, F32),
-            pltpu.VMEM(rel_bias.shape, F32),
+            pltpu.VMEM(rel_by_row.shape, F32),
             pltpu.VMEM((layers, heads * rows, keys), F32),
             dma((4 + 4 * layers,)),
             dma((layers, n_tp)),
@@ -259,9 +259,9 @@
             dma((2,)),
         ],
         compiler_params=pltpu.CompilerParams(
-            collective_id=0, has_side_effects=True, vmem_limit_bytes=48 * 1024 * 1024
+            collective_id=0, has_side_effects=True, vmem_limit_bytes=67043328
         ),
-    )(tokens, segment_ids.reshape(1, rows), gains, w_query, w_key, w_value, w_out, rel_bias)
+    )(tokens, segment_ids.reshape(1, rows), gains, w_query, w_key, w_value, w_out, rel_by_row)
 
 
 def solution(mesh):

time: 55.5 us -> 51.2 us (0.923)
  local copies, waits for them, and re-layouts: 5.73 us -> 1.38 us
    unnamed x16 -> x1, local copies, waits for them, and re-layouts: 5.73 us -> 1.38 us
where the time goes in v1:
time: 51.2 us; the launch traced here: 51.1 us
  Pallas kernels  49.7 us (97%)
  local copies, waits for them, and re-layouts  1.38 us (3%)
    pallas_call x1, Pallas kernels, on_device(): pl.pallas_call(functools.partial(kernel, n_sp, n_tp), out_shape=jax.Shape...  49.7 us
    unnamed x1, local copies, waits for them, and re-layouts  1.38 us

profile of v1, /device:TPU:1, one launch (start us, length us, event | category | flops | bytes accessed | tf_op | source)
XLA Modules:
  0.0 51.1 jit_solution(5470381262643698084)
XLA Ops:
  0.0 49.7 %shard_map.82 = bf16[128,128]{1,0:T(8,128)(2,1)} custom-call(bf16[128,128]{1,0:T(8,128)(2,1)} %tok.1, s32[1,128]{1,0:T(1,128)} %bitcast.3, f32[2,1024]{1,0:T(2,128)} %gains.1, bf16[2,256,128]{2,1,0:T(8,128)(2,1)} %wq.1, bf16[2,256,128]{2,1,0:T(8,128)(2,1)} %wk.1, bf16[2,256,128]{2,1,0:T(8,128)(2,1)} %wv.1, bf16[2,128,256]{2,1,0:T(8,128)(2,1)} %wo.1, ...), custom_call_target="tpu_custom_call" | custom-call | tf_op jit(solution)/shard_map/pallas_call | solution.py:230
  49.7 1.4 %copy.10 = bf16[128,128]{1,0:T(8,128)(2,1)} copy(bf16[128,128]{1,0:T(8,128)(2,1)} %shard_map.82) | data formatting | bytes 65536

commit v2 on v1

--- a/solution.py
+++ b/solution.py
@@ -29,7 +29,7 @@
 def kernel(
     n_sp, n_tp, tok, seg, gains, wq, wk, wv, wo, rel, out,
     xbuf, wbuf, wobuf, kvbuf, part, rsbuf, cur, docbuf, gbuf, relbuf, biasbuf,
-    local_sem, x_send, x_recv, w_send, w_recv, o_send, o_recv, h_send, h_recv, r_send, r_recv, d_send, d_recv,
+    local_sem, x_send, x_recv, w_send, w_recv, o_send, o_recv, h_send, h_recv, r_send, r_recv, d_send, d_recv, e_send, e_recv, f_send, f_recv,
 ):
     s, t = lax.axis_index("sp"), lax.axis_index("tp")
     layers = wbuf.shape[0]
@@ -46,7 +46,7 @@
         pltpu.make_async_copy(seg, docbuf.at[1], local_sem.at[0]),
         pltpu.make_async_copy(gains, gbuf, local_sem.at[1]),
         pltpu.make_async_copy(rel, relbuf, local_sem.at[2]),
-        pltpu.make_async_copy(tok, xbuf.at[0, t], local_sem.at[3]),
+        pltpu.make_async_copy(tok, xbuf.at[0, t, pl.ds(halo, rows)], local_sem.at[3]),
     ]
     weights = (wq, wk, wv)
     for l in range(layers):
@@ -64,7 +64,7 @@
     pl.semaphore_wait(barrier, n_tp + n_sp - 2)
 
     def x_copy(l, slot, peer):
-        return remote(tok if l == 0 else cur, xbuf.at[l, slot], x_send.at[l, peer], x_recv.at[l, slot], (s, peer))
+        return remote(tok if l == 0 else cur, xbuf.at[l, slot, pl.ds(halo, rows)], x_send.at[l, peer], x_recv.at[l, slot], (s, peer))
 
     def w_copy(l, j, slot, peer):
         return remote(weights[j].at[l], wbuf.at[l, j, slot], w_send.at[l, j, peer], w_recv.at[l, j, slot], (peer, t))
@@ -86,17 +86,36 @@
     def r_copy(l, peer, slot):
         return remote(part.at[l, peer], rsbuf.at[l, slot], r_send.at[l, peer], r_recv.at[l, slot], (s, peer))
 
+    edges = (
+        remote(
+            tok.at[pl.ds(rows - halo, halo)], xbuf.at[0, t, pl.ds(0, halo)],
+            e_send.at[0], e_recv.at[0], (following, t),
+        ),
+        remote(
+            tok.at[pl.ds(0, halo)], xbuf.at[0, t, pl.ds(rows + halo, halo)],
+            e_send.at[1], e_recv.at[1], (prev, t),
+        ),
+    )
+
+    def edge_copy(slot, side, peer):
+        piece = xbuf.at[0, slot, pl.ds(side * (rows + halo), halo)]
+        return remote(piece, piece, f_send.at[peer, side], f_recv.at[slot, side], (s, peer))
+
     docs = (
         remote(seg, docbuf.at[0], d_send.at[0], d_recv.at[0], (following, t)),
         remote(seg, docbuf.at[2], d_send.at[1], d_recv.at[1], (prev, t)),
     )
+    for copy in edges + docs:
+        copy.start()
     for peer in tp_peers:
         x_copy(0, t, peer).start()
     for j in (1, 2, 0):
         for peer in sp_peers:
             w_copy(0, j, s, peer).start()
-    for copy in docs:
-        copy.start()
+    for side in range(2):
+        edges[side].wait_recv()
+        for peer in tp_peers:
+            edge_copy(t, side, peer).start()
 
     local[0].wait()
     local[1].wait()
@@ -136,7 +155,14 @@
     for l in range(layers):
         for peer in tp_peers:
             x_copy(l, peer, peer).wait_recv()
-        pieces = [xbuf[l, i].astype(F32) for i in range(n_tp)]
+        if l == 0:
+            for side in range(2):
+                for peer in tp_peers:
+                    edge_copy(peer, side, peer).wait_recv()
+            first, count = 0, keys
+        else:
+            first, count = halo, rows
+        pieces = [xbuf[l, i, pl.ds(first, count)].astype(F32) for i in range(n_tp)]
         square = sum(piece * piece for piece in pieces)
         mean_sq = jnp.sum(square, axis=-1, keepdims=True) / (n_tp * feat)
         inv = lax.rsqrt(mean_sq + norm_eps)
@@ -146,21 +172,21 @@
             axis=1,
         )
 
-        def project(j):
+        def project(j, features):
             for peer in sp_peers:
                 w_copy(l, j, peer, peer).wait_recv()
             weight = wbuf[l, j].reshape(n_tp * feat, feat)
-            return jnp.dot(normed, weight, preferred_element_type=F32).astype(BF16)
-
-        kvbuf[l, 0, pl.ds(halo, rows)] = project(1)
-        kvbuf[l, 1, pl.ds(halo, rows)] = project(2)
-        halos = halo_copies(l)
+            return jnp.dot(features, weight, preferred_element_type=F32).astype(BF16)
+
+        kvbuf[l, 0, pl.ds(first, count)] = project(1, normed)
+        kvbuf[l, 1, pl.ds(first, count)] = project(2, normed)
+        halos = halo_copies(l) if l else ()
         for copy in halos:
             copy.start()
         if l == 0:
             for peer in sp_peers:
                 o_copy(0, s, peer).start()
-        query = project(0) * jnp.asarray(HEAD_DIM**-0.5, BF16)
+        query = project(0, normed[halo - first : halo - first + rows]) * jnp.asarray(HEAD_DIM**-0.5, BF16)
         head_of = lax.broadcasted_iota(jnp.int32, (rows, feat), 1) // HEAD_DIM
         query = jnp.concatenate([jnp.where(head_of == h, query, jnp.zeros_like(query)) for h in range(heads)], axis=0)
         for copy in halos:
@@ -199,7 +225,7 @@
             cur[...] = summed.astype(BF16)
             for peer in tp_peers:
                 x_copy(l + 1, t, peer).start()
-            xbuf[l + 1, t] = summed.astype(BF16)
+            xbuf[l + 1, t, pl.ds(halo, rows)] = summed.astype(BF16)
         else:
             out[...] = summed.astype(BF16)
 
@@ -208,12 +234,15 @@
     for l in range(layers):
         for peer in tp_peers:
             x_copy(l, t, peer).wait_send()
+            if l == 0:
+                for side in range(2):
+                    edge_copy(t, side, peer).wait_send()
             r_copy(l, peer, t).wait_send()
         for peer in sp_peers:
             for j in range(3):
                 w_copy(l, j, s, peer).wait_send()
             o_copy(l, s, peer).wait_send()
-        for copy in halo_copies(l):
+        for copy in halo_copies(l) if l else edges:
             copy.wait_send()
 
 
@@ -233,7 +262,7 @@
         in_specs=[anywhere] * 8,
         out_specs=pl.BlockSpec(memory_space=pltpu.VMEM),
         scratch_shapes=[
-            pltpu.VMEM((layers, n_tp, rows, feat), BF16),
+            pltpu.VMEM((layers, n_tp, keys, feat), BF16),
             pltpu.VMEM((layers, 3, n_sp, depth, feat), BF16),
             pltpu.VMEM((layers, n_sp, feat, width), BF16),
             pltpu.VMEM((layers, 2, keys, feat), BF16),
@@ -257,6 +286,10 @@
             dma((layers, n_tp)),
             dma((2,)),
             dma((2,)),
+            dma((2,)),
+            dma((2,)),
+            dma((n_tp, 2)),
+            dma((n_tp, 2)),
         ],
         compiler_params=pltpu.CompilerParams(
             collective_id=0, has_side_effects=True, vmem_limit_bytes=67043328

time: 51.2 us -> 52.5 us (1.025)
  Pallas kernels: 49.7 us -> 51 us
    pallas_call x1, Pallas kernels: 49.7 us -> 51 us  [on_device(): pl.pallas_call(functools.partial(kernel, n_sp, n_tp), out_shape=jax.Shape...]
where the time goes in v2:
time: 52.5 us; the launch traced here: 52.4 us
  Pallas kernels  51 us (97%)
  local copies, waits for them, and re-layouts  1.38 us (3%)
    pallas_call x1, Pallas kernels, on_device(): pl.pallas_call(functools.partial(kernel, n_sp, n_tp), out_shape=jax.Shape...  51 us
    unnamed x1, local copies, waits for them, and re-layouts  1.38 us

profile of v2, /device:TPU:1, one launch (start us, length us, event | category | flops | bytes accessed | tf_op | source)
XLA Modules:
  0.0 52.4 jit_solution(16879938401261255607)
XLA Ops:
  0.0 51.0 %shard_map.82 = bf16[128,128]{1,0:T(8,128)(2,1)} custom-call(bf16[128,128]{1,0:T(8,128)(2,1)} %tok.1, s32[1,128]{1,0:T(1,128)} %bitcast.3, f32[2,1024]{1,0:T(2,128)} %gains.1, bf16[2,256,128]{2,1,0:T(8,128)(2,1)} %wq.1, bf16[2,256,128]{2,1,0:T(8,128)(2,1)} %wk.1, bf16[2,256,128]{2,1,0:T(8,128)(2,1)} %wv.1, bf16[2,128,256]{2,1,0:T(8,128)(2,1)} %wo.1, ...), custom_call_target="tpu_custom_call" | custom-call | tf_op jit(solution)/shard_map/pallas_call | solution.py:259
  51.0 1.4 %copy.10 = bf16[128,128]{1,0:T(8,128)(2,1)} copy(bf16[128,128]{1,0:T(8,128)(2,1)} %shard_map.82) | data formatting | bytes 65536

commit v3 on v1

--- a/solution.py
+++ b/solution.py
@@ -40,6 +40,9 @@
     grid_rows = rows // GRID_W
     prev, following = lax.rem(s + n_sp - 1, n_sp), lax.rem(s + 1, n_sp)
     tp_peers = [lax.rem(t + k, n_tp) for k in range(1, n_tp)]
+    other = lambda i: i + 1 - 2 * lax.rem(i, 2)
+    partner = other(t)
+    mates = [lax.rem(t + k, n_tp) for k in range(2, n_tp, 2)]
     sp_peers = [lax.rem(s + k, n_sp) for k in range(1, n_sp)]
 
     local = [
@@ -66,6 +69,20 @@
     def x_copy(l, slot, peer):
         return remote(tok if l == 0 else cur, xbuf.at[l, slot], x_send.at[l, peer], x_recv.at[l, slot], (s, peer))
 
+    def x_forward(l, slot):
+        piece = xbuf.at[l, slot]
+        return remote(piece, piece, x_send.at[l, other(slot)], x_recv.at[l, slot], (s, partner))
+
+    def spread(l):
+        for mate in mates:
+            x_copy(l, t, mate).start()
+        x_copy(l, t, partner).start()
+
+    def pass_on(l):
+        for mate in mates:
+            x_copy(l, mate, mate).wait_recv()
+            x_forward(l, mate).start()
+
     def w_copy(l, j, slot, peer):
         return remote(weights[j].at[l], wbuf.at[l, j, slot], w_send.at[l, j, peer], w_recv.at[l, j, slot], (peer, t))
 
@@ -90,13 +107,14 @@
         remote(seg, docbuf.at[0], d_send.at[0], d_recv.at[0], (following, t)),
         remote(seg, docbuf.at[2], d_send.at[1], d_recv.at[1], (prev, t)),
     )
-    for peer in tp_peers:
-        x_copy(0, t, peer).start()
+    spread(0)
     for j in (1, 2, 0):
         for peer in sp_peers:
             w_copy(0, j, s, peer).start()
     for copy in docs:
         copy.start()
+
+    pass_on(0)
 
     local[0].wait()
     local[1].wait()
@@ -134,8 +152,10 @@
         copy.wait()
 
     for l in range(layers):
-        for peer in tp_peers:
-            x_copy(l, peer, peer).wait_recv()
+        if l:
+            pass_on(l)
+        for slot in [partner] + [other(mate) for mate in mates]:
+            x_copy(l, slot, slot).wait_recv()
         pieces = [xbuf[l, i].astype(F32) for i in range(n_tp)]
         square = sum(piece * piece for piece in pieces)
         mean_sq = jnp.sum(square, axis=-1, keepdims=True) / (n_tp * feat)
@@ -197,8 +217,7 @@
             summed = summed + rsbuf[l, peer].astype(F32)
         if l + 1 < layers:
             cur[...] = summed.astype(BF16)
-            for peer in tp_peers:
-                x_copy(l + 1, t, peer).start()
+            spread(l + 1)
             xbuf[l + 1, t] = summed.astype(BF16)
         else:
             out[...] = summed.astype(BF16)
@@ -207,8 +226,11 @@
         copy.wait_send()
     for l in range(layers):
         for peer in tp_peers:
-            x_copy(l, t, peer).wait_send()
             r_copy(l, peer, t).wait_send()
+        for mate in mates:
+            x_copy(l, t, mate).wait_send()
+            x_forward(l, mate).wait_send()
+        x_copy(l, t, partner).wait_send()
         for peer in sp_peers:
             for j in range(3):
                 w_copy(l, j, s, peer).wait_send()

time: 51.2 us -> 49.8 us (0.973)
  Pallas kernels: 49.7 us -> 48.1 us
    pallas_call x1, Pallas kernels: 49.7 us -> 48.1 us  [on_device(): pl.pallas_call(functools.partial(kernel, n_sp, n_tp), out_shape=jax.Shape...]
where the time goes in v3:
time: 49.8 us; the launch traced here: 49.5 us
  Pallas kernels  48.1 us (97%)
  local copies, waits for them, and re-layouts  1.38 us (3%)
    pallas_call x1, Pallas kernels, on_device(): pl.pallas_call(functools.partial(kernel, n_sp, n_tp), out_shape=jax.Shape...  48.1 us
    unnamed x1, local copies, waits for them, and re-layouts  1.38 us

profile of v3, /device:TPU:1, one launch (start us, length us, event | category | flops | bytes accessed | tf_op | source)
XLA Modules:
  0.0 49.5 jit_solution(585637922468646325)
XLA Ops:
  0.0 48.1 %shard_map.82 = bf16[128,128]{1,0:T(8,128)(2,1)} custom-call(bf16[128,128]{1,0:T(8,128)(2,1)} %tok.1, s32[1,128]{1,0:T(1,128)} %bitcast.3, f32[2,1024]{1,0:T(2,128)} %gains.1, bf16[2,256,128]{2,1,0:T(8,128)(2,1)} %wq.1, bf16[2,256,128]{2,1,0:T(8,128)(2,1)} %wk.1, bf16[2,256,128]{2,1,0:T(8,128)(2,1)} %wv.1, bf16[2,128,256]{2,1,0:T(8,128)(2,1)} %wo.1, ...), custom_call_target="tpu_custom_call" | custom-call | tf_op jit(solution)/shard_map/pallas_call | solution.py:252
  48.1 1.4 %copy.10 = bf16[128,128]{1,0:T(8,128)(2,1)} copy(bf16[128,128]{1,0:T(8,128)(2,1)} %shard_map.82) | data formatting | bytes 65536
